TPU v7x, 32 devices: a whole 2x2x4 slice. The times are simulated.
32 devices in a mesh: sp: 8 (over z, x), tp: 4 (over y, core).
Axes of the slice: x: 2, y: 2, z: 4, core: 2. Of those that a mesh axis runs over, the one named last changes fastest.
Arguments:
- residual: bfloat16 [1024, 2048], P('sp'), may hold values from -6 to 6
- queries: bfloat16 [1024, 2048], P('sp', 'tp'), may hold values from -6 to 6
- keys: bfloat16 [1024, 2048], P('sp', 'tp'), may hold values from -6 to 6
- values: bfloat16 [1024, 2048], P('sp', 'tp'), may hold values from -24 to 24
- stick_bias: bfloat16 [32, 1024], P('tp', 'sp'), may hold values from 2 to 13
- query_gain: float32 [64], replicated, may hold values from 0.1 to 1.9
- key_gain: float32 [64], replicated, may hold values from 0.1 to 1.9
- out_weight: bfloat16 [2048, 2048], P('tp'), may hold values from -0.25 to 0.25
- norm_gain: float32 [2048], replicated, may hold values from 0.1 to 1.9
- route_ids: int32 [1024, 2], P('sp'), may hold values from 0 to 7, all different within a row; in each aligned block of 128 rows (0 to 127, 128 to 255, ...) at most 40 rows name the same one
- route_weights: float32 [1024, 2], P('sp'), may hold values from 0.1 to 1
- gate_weight: bfloat16 [8, 2048, 2048], P('sp', None, 'tp'), may hold values from -3 to 3
- up_weight: bfloat16 [8, 2048, 2048], P('sp', None, 'tp'), may hold values from -3 to 3
- down_weight: bfloat16 [8, 2048, 2048], P('sp', 'tp'), may hold values from -0.125 to 0.125
Outputs:
- layer_out: bfloat16 [1024, 2048], P('sp', 'tp')
Inputs may be any that keep to these rules, and one draw needn't show every extreme that they name: `route_ids`: each row names 2 different experts. In every aligned block of 128 rows at most 40 rows name one expert, and in every draw some expert is named by exactly 40 rows of some block.
All inputs are finite; a program needn't handle non-finite values.
Results may differ from a plain program's by a relative error of at most 0.028.
Values may be sent and summed in bfloat16 or wider, within the bound.
A program may use at most 64 MiB of HBM per device.

v0:
```python
import math
import jax
import jax.numpy as jnp
from jax import lax
from jax.sharding import PartitionSpec as P

epsilon = 1e-06
clamp_limit = 7.0
swish_scale = 1.702


def head_normalize(packed, gain):
    values_f = packed.astype(jnp.float32).reshape(packed.shape[0], -1, gain.shape[0])
    scaled = (
        values_f * lax.rsqrt(jnp.mean(values_f * values_f, axis=-1, keepdims=True) + epsilon) * gain
    )
    return scaled.astype(jnp.bfloat16)


def activate(gate_pre, up_pre):
    gate_top = jnp.minimum(gate_pre, clamp_limit)
    up_clip = jnp.clip(up_pre, -clamp_limit, clamp_limit)
    return (up_clip + 1.0) * (gate_top * jax.nn.sigmoid(swish_scale * gate_top))


def slot_table(picked, expert_count, capacity):
    flat_ids = picked.reshape(-1)
    one_hot = (flat_ids[:, None] == jnp.arange(expert_count, dtype=jnp.int32)[None, :]).astype(
        jnp.int32
    )
    before = jnp.sum((jnp.cumsum(one_hot, axis=0) - one_hot) * one_hot, axis=1)
    return flat_ids * capacity + before


def key_block(state_pair, queries_n, keys_block, values_block, bias_block, first_key, query_pos):
    summed, log_carry = state_pair
    key_count = bias_block.shape[1]
    head_total = bias_block.shape[0]
    keys_heads = keys_block.reshape(key_count, head_total, -1)
    values_heads = values_block.reshape(key_count, head_total, -1)
    head_dim = keys_heads.shape[2]
    scores = jnp.einsum(
        "qhd,khd->hqk", queries_n, keys_heads, preferred_element_type=jnp.float32
    ) * head_dim ** (-0.5)
    scores = scores - bias_block.astype(jnp.float32)[:, None, :]
    key_pos = first_key + jnp.arange(key_count, dtype=jnp.int32)
    causal = ((key_pos[None, :] < query_pos[:, None]) & (key_pos[None, :] >= 0))[None]
    log_stay = jnp.where(causal, jax.nn.log_sigmoid(-scores), 0.0)
    later_sum = lax.cumsum(log_stay, axis=2, reverse=True) - log_stay
    weight = jnp.where(
        causal, jnp.exp(jax.nn.log_sigmoid(scores) + later_sum + log_carry[:, :, None]), 0.0
    )
    summed = summed + jnp.einsum(
        "hqk,khd->qhd",
        weight.astype(jnp.bfloat16),
        values_heads,
        preferred_element_type=jnp.float32,
    )
    return (summed, log_carry + jnp.sum(log_stay, axis=2))


def per_device(
    residual,
    queries,
    keys,
    values,
    stick_bias,
    query_gain,
    key_gain,
    out_weight,
    norm_gain,
    route_ids,
    route_weights,
    gate_weight,
    up_weight,
    down_weight,
):
    tok_rows = queries.shape[0]
    width_sp = lax.axis_size("sp")
    offset = lax.axis_index("sp") * tok_rows
    query_pos = offset + jnp.arange(tok_rows, dtype=jnp.int32)
    queries_n = head_normalize(queries, query_gain)
    keys_n = head_normalize(keys, key_gain).reshape(tok_rows, -1)
    head_total = stick_bias.shape[0]
    head_dim = query_gain.shape[0]
    state_pair = (
        jnp.zeros((tok_rows, head_total, head_dim), jnp.float32),
        jnp.zeros((head_total, tok_rows), jnp.float32),
    )
    all_keys, all_values, all_bias = (
        lax.all_gather(keys_n, "sp", axis=0, tiled=True),
        lax.all_gather(values, "sp", axis=0, tiled=True),
        lax.all_gather(stick_bias, "sp", axis=1, tiled=True),
    )
    key_total = all_keys.shape[0]
    block_len = math.gcd(key_total, 512)
    block_total = key_total // block_len

    def sweep_block(block_step, running):
        first_key = (block_total - 1 - block_step) * block_len
        return key_block(
            running,
            queries_n,
            lax.dynamic_slice_in_dim(all_keys, first_key, block_len, 0),
            lax.dynamic_slice_in_dim(all_values, first_key, block_len, 0),
            lax.dynamic_slice_in_dim(all_bias, first_key, block_len, 1),
            first_key,
            query_pos,
        )

    state_pair = lax.fori_loop(0, block_total, sweep_block, state_pair)
    attended = state_pair[0].reshape(tok_rows, head_total * head_dim).astype(jnp.bfloat16)
    partial_value = jnp.dot(attended, out_weight, preferred_element_type=jnp.float32)
    model_width = residual.shape[1]
    expert_count = width_sp * gate_weight.shape[0]
    pick_count = route_ids.shape[1]
    capacity = (5 * tok_rows * pick_count + 4 * expert_count - 1) // (4 * expert_count)
    slot_index = slot_table(route_ids, expert_count, capacity)
    assigned = slot_index.shape[0]
    source = (
        jnp.zeros((expert_count * capacity,), jnp.int32)
        .at[slot_index]
        .set(jnp.arange(assigned, dtype=jnp.int32) // pick_count)
    )
    filled = (
        jnp.zeros((expert_count * capacity,), jnp.bfloat16)
        .at[slot_index]
        .set(jnp.ones((assigned,), jnp.bfloat16))
    )
    gate_local = gate_weight[0]
    up_local = up_weight[0]
    down_local = down_weight[0]
    mixed_share = lax.psum_scatter(
        partial_value.astype(jnp.bfloat16), "tp", scatter_dimension=1, tiled=True
    ).astype(jnp.float32)
    own_width = mixed_share.shape[1]
    col_start = lax.axis_index("tp") * own_width
    own_res = lax.dynamic_slice_in_dim(residual, col_start, own_width, 1).astype(jnp.float32)
    own_cols = (own_res + mixed_share).astype(jnp.bfloat16).astype(jnp.float32)
    square_total = lax.psum(jnp.sum(own_cols * own_cols, axis=1), "tp")
    gain_cols = lax.dynamic_slice_in_dim(norm_gain, col_start, own_width, 0)
    normed_share = (
        own_cols * lax.rsqrt(square_total / model_width + epsilon)[:, None] * gain_cols
    ).astype(jnp.bfloat16)
    outgoing = (normed_share[source] * filled[:, None]).reshape(expert_count, capacity, -1)
    piece = lax.all_gather(
        lax.all_to_all(outgoing, "sp", split_axis=0, concat_axis=0, tiled=True),
        "tp",
        axis=2,
        tiled=True,
    )
    gate_pre = jnp.einsum("scd,df->scf", piece, gate_local, preferred_element_type=jnp.float32)
    up_pre = jnp.einsum("scd,df->scf", piece, up_local, preferred_element_type=jnp.float32)
    hidden = activate(gate_pre, up_pre).astype(jnp.bfloat16)
    share = jnp.einsum("scf,fd->scd", hidden, down_local, preferred_element_type=jnp.float32)
    returned = lax.psum_scatter(share.astype(jnp.bfloat16), "tp", scatter_dimension=2, tiled=True)
    arrived = lax.all_to_all(returned, "sp", split_axis=0, concat_axis=0, tiled=True)
    columns = arrived.shape[2]
    taken_rows = arrived.reshape(expert_count * capacity, columns)[slot_index]
    taken_rows = taken_rows.astype(jnp.float32).reshape(tok_rows, pick_count, columns)
    routed = jnp.sum(taken_rows * route_weights[:, :, None], axis=1)
    return (own_cols + routed).astype(jnp.bfloat16)


def solution(mesh):
    placed = (
        P("sp", None),
        P("sp", "tp"),
        P("sp", "tp"),
        P("sp", "tp"),
        P("tp", "sp"),
        P(),
        P(),
        P("tp", None),
        P(),
        P("sp", None),
        P("sp", None),
        P("sp", None, "tp"),
        P("sp", None, "tp"),
        P("sp", "tp", None),
    )
    return jax.shard_map(
        per_device, mesh=mesh, in_specs=placed, out_specs=P("sp", "tp"), check_vma=False
    )
```

profile of v0, /device:TPU:0, one launch (start us, length us, event | category | flops | bytes accessed | tf_op | source)
XLA Modules:
  0.0 249.5 jit_solution(2540238676448930279)
XLA Ops:
  6.5 1.2 copy.26
  7.8 0.7 mul.146
  8.4 0.1 mul.147
  8.5 0.8 fusion.52
  9.3 0.0 all-gather.6.cloned.1.call-update
  9.3 0.0 all-gather.4.cloned.1.call-start
  9.4 1.7 copy.25
  11.1 0.0 reduce-scatter.3.cloned.1.call-start
  11.1 1.0 copy.27
  12.1 0.8 copy.29
  12.9 0.1 eq.29
  13.1 0.6 reduce-window.24
  13.7 28.2 %all_gather.14 = bf16[8,1024]{1,0:T(8,128)(2,1)S(1)} all-gather(bf16[8,128]{1,0:T(8,128)(2,1)} %param.20), channel_id=1, replica_groups=mesh['sp'=8,'tp'=4] {'sp'}, dimensions={1}, use_global_device_ids=true | all-gather | bytes 18432 | tf_op jit(solution)/shard_map/all_gather | solution.py:93
  42.0 0.7 multiply_convert_fusion
  42.7 8.9 %all-gather.6.cloned.1.call-done = bf16[1024,512]{0,1:T(8,128)(2,1)} async-done(((bf16[128,512]{0,1:T(8,128)(2,1)}), bf16[1024,512]{0,1:T(8,128)(2,1)}) %all-gather.6.cloned.1.call-update) | async-done | bytes 1048592 | tf_op jit(solution)/shard_map/all_gather | solution.py:91
  51.6 40.3 %all-gather.4.cloned.1.call-done = bf16[1024,512]{0,1:T(8,128)(2,1)} async-done(((bf16[128,512]{0,1:T(8,128)(2,1)}), bf16[1024,512]{0,1:T(8,128)(2,1)}) %all-gather.4.cloned.1.call-update) | async-done | bytes 1048592 | tf_op jit(solution)/shard_map/all_gather | solution.py:92
  91.9 33.3 %while.16 = (s32[]{:T(128)}, f32[128,8,64]{0,2,1:T(8,128)S(1)}, f32[8,128]{1,0:T(8,128)S(1)}, bf16[1024,512]{0,1:T(8,128)(2,1)}, bf16[1024,512]{0,1:T(8,128)(2,1...) while((s32[]{:T(128)}, f32[128,8,64]{0,2,1:T(8,128)S(1)}, ...), condition=%wide.region_6.7_spmd.clone, body=%wide.region_2.6_spmd.clone.sunk | while | flops 219436672 | bytes 27240652 | solution.py:111
  91.9 1.3 constant_dynamic-slice_fusion.3
  93.2 0.2 compare_and_fusion.2
  93.4 3.0 %fusion.93 = (f32[8,128]{1,0:T(8,128)S(1)}, f32[8,128,512]{1,2,0:T(8,128)S(1)}, f32[8,512,128]{2,1,0:T(8,128)}) fusion(f32[8,512]{1,0:T(8,128)S(1)} %dynamic-slice_convert_fusion.2, pred[128,512]{0,1:T(8,128)(4,1)S(1)} %compare_and_fusion.2, bf16[512,8,64]{0,2,1:T(8,128)(2,1)S(1)} %bitcast.116, bf16[128,8,64]{0,2,1:T(8,128)(2,1)S(1)} %get-tuple-element.292), kind=kOutput, calls=%fused_computation.39.clone.1 | convolution fusion | flops 72875008 | bytes 4935680 | tf_op jit(solution)/shard_map/while/body/eval_jaxpr/qhd,khd->hqk/dot_general | solution.py:42
  96.4 5.0 %fusion.94 = f32[8,128,4,128]{1,0,3,2:T(8,128)S(1)} fusion(f32[8,128,4,128]{1,3,2,0:T(8,128)S(1)} %bitcast.114), kind=kOutput, calls=%fused_computation.23.clone.1 | output fusion | flops 66584576 | bytes 4194304 | tf_op jit(solution)/shard_map/reduce-window.6
  101.5 0.1 broadcast_add_fusion.2
  101.6 1.7 copy.38
  103.3 4.8 %fusion.97 = bf16[8,128,512]{1,2,0:T(8,128)(2,1)S(1)} fusion(f32[8,128,4,128]{1,3,2,0:T(8,128)} %copy.38, f32[8,512,128]{2,1,0:T(8,128)} %get-tuple-element.259, f32[8,128]{1,0:T(8,128)S(1)} %get-tuple-element.261, f32[8,512]{1,0:T(8,128)S(1)} %dynamic-slice_convert_fusion.2, pred[128,512]{0,1:T(8,128)(4,1)S(1)} %compare_and_fusion.2), kind=kLoop, calls=%fused_computation.12.clone.1 | loop fusion | flops 12058624 | bytes 5328896 | tf_op jit(solution)/shard_map/while/body/eval_jaxpr/convert_element_type | solution.py:55
  108.1 0.3 fusion.98
  108.5 1.3 constant_dynamic-slice_fusion.3
  109.8 0.2 compare_and_fusion.2
  110.1 3.0 %fusion.93 = (f32[8,128]{1,0:T(8,128)S(1)}, f32[8,128,512]{1,2,0:T(8,128)S(1)}, f32[8,512,128]{2,1,0:T(8,128)}) fusion(f32[8,512]{1,0:T(8,128)S(1)} %dynamic-slice_convert_fusion.2, pred[128,512]{0,1:T(8,128)(4,1)S(1)} %compare_and_fusion.2, bf16[512,8,64]{0,2,1:T(8,128)(2,1)S(1)} %bitcast.116, bf16[128,8,64]{0,2,1:T(8,128)(2,1)S(1)} %get-tuple-element.292), kind=kOutput, calls=%fused_computation.39.clone.1 | convolution fusion | flops 72875008 | bytes 4935680 | tf_op jit(solution)/shard_map/while/body/eval_jaxpr/qhd,khd->hqk/dot_general | solution.py:42
  113.1 5.0 %fusion.94 = f32[8,128,4,128]{1,0,3,2:T(8,128)S(1)} fusion(f32[8,128,4,128]{1,3,2,0:T(8,128)S(1)} %bitcast.114), kind=kOutput, calls=%fused_computation.23.clone.1 | output fusion | flops 66584576 | bytes 4194304 | tf_op jit(solution)/shard_map/reduce-window.6
  118.1 0.1 broadcast_add_fusion.2
  118.3 1.7 copy.38
  120.0 4.8 %fusion.97 = bf16[8,128,512]{1,2,0:T(8,128)(2,1)S(1)} fusion(f32[8,128,4,128]{1,3,2,0:T(8,128)} %copy.38, f32[8,512,128]{2,1,0:T(8,128)} %get-tuple-element.259, f32[8,128]{1,0:T(8,128)S(1)} %get-tuple-element.261, f32[8,512]{1,0:T(8,128)S(1)} %dynamic-slice_convert_fusion.2, pred[128,512]{0,1:T(8,128)(4,1)S(1)} %compare_and_fusion.2), kind=kLoop, calls=%fused_computation.12.clone.1 | loop fusion | flops 12058624 | bytes 5328896 | tf_op jit(solution)/shard_map/while/body/eval_jaxpr/convert_element_type | solution.py:55
  124.8 0.3 fusion.98
  125.2 2.9 %convolution_convert_fusion.1 = bf16[128,2048]{1,0:T(8,128)(2,1)} fusion(bf16[128,512]{0,1:T(8,128)(2,1)S(1)} %bitcast.118, bf16[512,2048]{1,0:T(8,128)(2,1)} %param.23), kind=kOutput, calls=%fused_computation.41 | convolution fusion | flops 268697600 | bytes 2752512 | tf_op jit(solution)/shard_map/dot_general | solution.py:113
  128.1 0.0 all-gather.8.cloned.1.call-start
  128.1 0.2 slice_reduce_fusion
  128.3 0.1 eq.25
  128.5 0.1 copy.28
  128.6 0.1 mul.162
  128.8 0.1 fusion.58
  128.9 1.4 scatter_custom_fusion
  130.3 2.2 scatter_custom_fusion.1
  132.5 0.1 mul.164
  132.6 0.8 dynamic_slice.28
  133.3 15.6 %reduce-scatter.3.cloned.1.call-done = bf16[128,512]{1,0:T(8,128)(2,1)} async-done(((bf16[128,2048]{1,0:T(8,128)(2,1)}), bf16[128,512]{1,0:T(8,128)(2,1)}) %reduce-scatter.3.cloned.1.call-update) | async-done | bytes 131088 | tf_op jit(solution)/shard_map/reduce_scatter | solution.py:133
  148.9 1.1 fusion.53
  150.0 5.8 %psum.7 = f32[128]{0:T(128)S(1)} all-reduce(f32[128]{0:T(128)S(1)} %get-tuple-element.193), channel_id=1, replica_groups=mesh['sp'=8,'tp'=4] {'tp'}, use_global_device_ids=true, to_apply=%region_9.10 | all-reduce | flops 128 | bytes 1024 | tf_op jit(solution)/shard_map/psum | solution.py:140
  155.8 0.1 fusion.55
  155.9 2.0 gather_fusion
  157.9 0.1 broadcast_multiply_fusion
  158.0 16.3 %all_to_all.10 = bf16[8,40,512]{2,1,0:T(8,128)(2,1)} all-to-all(bf16[8,40,512]{2,1,0:T(8,128)(2,1)S(1)} %broadcast_multiply_fusion), channel_id=1, replica_groups=mesh['sp'=8,'tp'=4] {'sp'}, dimensions={0} | all-to-all | bytes 655360 | tf_op jit(solution)/shard_map/all_to_all | solution.py:147
  174.3 0.0 all-gather.8.cloned.1.call-update
  174.4 0.2 reduce-scatter.5.cloned.1.call-start
  174.6 15.6 %all-gather.8.cloned.1.call-done = bf16[8,40,2048]{2,1,0:T(8,128)(2,1)} async-done(((bf16[8,40,512]{2,1,0:T(8,128)(2,1)}), bf16[8,40,2048]{2,1,0:T(8,128)(2,1)}) %all-gather.8.cloned.1.call-update) | async-done | bytes 1310736 | tf_op jit(solution)/shard_map/all_gather | solution.py:146
  190.1 2.8 %fusion.33 = f32[8,40,512]{2,1,0:T(8,128)S(1)} fusion(bf16[8,40,2048]{2,1,0:T(8,128)(2,1)} %all-gather.8.cloned.1.call-done, bf16[1,2048,512]{2,1,0:T(8,128)(2,1)} %param.27), kind=kOutput, calls=%fused_computation.50 | convolution fusion | flops 671252480 | bytes 4063232 | tf_op jit(solution)/shard_map/scd,df->scf/dot_general | solution.py:152
  193.0 4.8 %convolution_convert_fusion = bf16[8,40,2048]{2,1,0:T(8,128)(2,1)} fusion(bf16[1,512,2048]{2,1,0:T(8,128)(2,1)S(1)} %copy-done, bf16[8,40,2048]{2,1,0:T(8,128)(2,1)} %all-gather.8.cloned.1.call-done, bf16[1,2048,512]{2,1,0:T(8,128)(2,1)} %param.28, f32[8,40,512]{2,1,0:T(8,128)S(1)} %fusion.33), kind=kOutput, calls=%fused_computation.40 | convolution fusion | flops 1344307200 | bytes 7471104 | tf_op jit(solution)/shard_map/scf,fd->scd/dot_general | solution.py:155
  197.8 26.6 %reduce-scatter.5.cloned.1.call-done = bf16[8,40,512]{2,1,0:T(8,128)(2,1)} async-done(((bf16[8,40,2048]{2,1,0:T(8,128)(2,1)}), bf16[8,40,512]{2,1,0:T(8,128)(2,1)}) %reduce-scatter.5.cloned.1.call-update) | async-done | bytes 327696 | tf_op jit(solution)/shard_map/reduce_scatter | solution.py:156
  224.4 5.5 %all-to-all-start.1 = ((bf16[8,40,512]{2,1,0:T(8,128)(2,1)}), bf16[8,40,512]{2,1,0:T(8,128)(2,1)S(1)}, u32[]{:S(2)}, u32[]{:S(2)}) async-start(bf16[8,40,512]{2,1,0:T(8,128)(2,1)} %reduce-scatter.5.cloned.1.call-done), calls=%async_computation.3 | async-start | bytes 655360 | tf_op jit(solution)/shard_map/all_to_all | solution.py:157
  229.9 0.1 copy.31
  230.0 10.0 %all-to-all-done.1 = bf16[8,40,512]{2,1,0:T(8,128)(2,1)S(1)} async-done(((bf16[8,40,512]{2,1,0:T(8,128)(2,1)}), bf16[8,40,512]{2,1,0:T(8,128)(2,1)S(1)}, u32[]{:S(2)}, u32[]{:S(2)}) %all-to-all-start.1) | async-done | bytes 327712 | tf_op jit(solution)/shard_map/all_to_all | solution.py:157
  240.1 1.2 gather_fusion.1
  241.2 0.3 reshape.188
  241.5 0.7 multiply_reduce_fusion
  242.3 0.7 fusion.56
  (42 shorter events, 0.3 us)
Async XLA Ops:
  6.5 186.5 %copy-start = (bf16[1,512,2048]{2,1,0:T(8,128)(2,1)S(1)}, bf16[1,512,2048]{2,1,0:T(8,128)(2,1)}, u32[]{:S(2)}) copy-start(bf16[1,512,2048]{2,1,0:T(8,128)(2,1)} %param.29) | copy-start | bytes 6291460
  6.5 45.1 %all-gather.6.cloned.1.call-start = ((), (), s32[]{:S(2)}) async-start(), calls=%async_computation.5 | async-start | bytes 1179648 | tf_op jit(solution)/shard_map/all_gather | solution.py:91
  9.3 82.6 %all-gather.4.cloned.1.call-start = ((), (), s32[]{:S(2)}) async-start(), calls=%async_computation.4 | async-start | bytes 1179648 | tf_op jit(solution)/shard_map/all_gather | solution.py:92
  11.1 137.9 %reduce-scatter.3.cloned.1.call-start = ((), (), s32[]{:S(2)}) async-start(), calls=%async_computation.6 | async-start | bytes 655360 | tf_op jit(solution)/shard_map/reduce_scatter | solution.py:133
  125.1 3.4 %copy-start.1 = (s32[128,2]{0,1:T(2,128)S(1)}, s32[128,2]{0,1:T(2,128)}, u32[]{:S(2)}) copy-start(s32[128,2]{0,1:T(2,128)} %param.25) | copy-start | bytes 3076
  128.1 62.1 %all-gather.8.cloned.1.call-start = ((), (), s32[]{:S(2)}) async-start(), calls=%async_computation.7 | async-start | bytes 1638400 | tf_op jit(solution)/shard_map/all_gather | solution.py:146
  174.4 50.0 %reduce-scatter.5.cloned.1.call-start = ((), (), s32[]{:S(2)}) async-start(), calls=%async_computation.8 | async-start | bytes 1638400 | tf_op jit(solution)/shard_map/reduce_scatter | solution.py:156
  193.0 36.9 %copy-start.2 = (f32[128,2]{0,1:T(2,128)S(1)}, f32[128,2]{0,1:T(2,128)}, u32[]{:S(2)}) copy-start(f32[128,2]{0,1:T(2,128)} %param.26) | copy-start | bytes 3076
  224.4 15.7 %all-to-all-start.1 = ((bf16[8,40,512]{2,1,0:T(8,128)(2,1)}), bf16[8,40,512]{2,1,0:T(8,128)(2,1)S(1)}, u32[]{:S(2)}, u32[]{:S(2)}) async-start(bf16[8,40,512]{2,1,0:T(8,128)(2,1)} %reduce-scatter.5.cloned.1.call-done), calls=%async_computation.3 | async-start | bytes 655360 | tf_op jit(solution)/shard_map/all_to_all | solution.py:157
Sparse Core Ops, SparseCore 0:
  9.4 42.1 all-gather.5
  53.6 38.1 all-gather.3
  128.2 20.6 reduce-scatter.2
  174.5 15.6 all-gather.7
  197.9 26.4 reduce-scatter.4
where the time goes:
time: 250 us; the launch traced here: 249 us
  waiting for transfers between devices  117 us (47%)
  blocking collectives  50.3 us (20%)
  other arithmetic  25.5 us (10%)
  local copies, waits for them, and re-layouts  20.1 us (8%)
  matrix products  17.2 us (7%)
  between operations  13.4 us (5%)
  starting transfers between devices  5.86 us (2%)
    all_gather x1, waiting for transfers between devices, per_device(): lax.all_gather(values, 'sp', axis=0, tiled=True)  40.3 us
    all_gather x1, blocking collectives, per_device(): lax.all_gather(stick_bias, 'sp', axis=1, tiled=True)  28.2 us
    reduce_scatter x1, waiting for transfers between devices, per_device(): lax.psum_scatter(share.astype(jnp.bfloat16), 'tp', scatter_dimension=2, t...  26.6 us
    all_to_all x1, blocking collectives, per_device(): lax.all_to_all(outgoing, 'sp', split_axis=0, concat_axis=0, tiled=True)  16.3 us
    reduce_scatter x1, waiting for transfers between devices, per_device(): lax.psum_scatter(partial_value.astype(jnp.bfloat16), 'tp', scatter_dimens...  15.6 us
    all_gather x1, waiting for transfers between devices, per_device(): lax.all_gather(lax.all_to_all(outgoing, 'sp', split_axis=0, concat_axis=0...  15.6 us
    another operation x6, other arithmetic  10.7 us
    all_to_all x1, waiting for transfers between devices, per_device(): lax.all_to_all(returned, 'sp', split_axis=0, concat_axis=0, tiled=True)  10 us
  transfers between devices with their start and end apart: 6, of which 6 were waited for; matrix products, arithmetic and copies ran while one was open for 4% of the time, Pallas kernels for 0%

commit v1 on v0

--- a/solution.py
+++ b/solution.py
@@ -143,12 +143,9 @@
         own_cols * lax.rsqrt(square_total / model_width + epsilon)[:, None] * gain_cols
     ).astype(jnp.bfloat16)
     outgoing = (normed_share[source] * filled[:, None]).reshape(expert_count, capacity, -1)
-    piece = lax.all_gather(
-        lax.all_to_all(outgoing, "sp", split_axis=0, concat_axis=0, tiled=True),
-        "tp",
-        axis=2,
-        tiled=True,
-    )
+    sheet = lax.all_to_all(outgoing, "sp", split_axis=0, concat_axis=0, tiled=True)
+    d_next = lax.all_gather(sheet, "tp")
+    piece = jnp.concatenate(d_next, axis=2)
     gate_pre = jnp.einsum("scd,df->scf", piece, gate_local, preferred_element_type=jnp.float32)
     up_pre = jnp.einsum("scd,df->scf", piece, up_local, preferred_element_type=jnp.float32)
     hidden = activate(gate_pre, up_pre).astype(jnp.bfloat16)

time: 250 us -> 251 us (level)
  no operation moved by 1% of the time
where the time goes in v1:
time: 251 us; the launch traced here: 250 us
  waiting for transfers between devices  117 us (47%)
  blocking collectives  50.3 us (20%)
  other arithmetic  25.5 us (10%)
  local copies, waits for them, and re-layouts  22 us (9%)
  matrix products  15.8 us (6%)
  between operations  13.4 us (5%)
  starting transfers between devices  5.86 us (2%)
    all_gather x1, waiting for transfers between devices, per_device(): lax.all_gather(values, 'sp', axis=0, tiled=True)  40.3 us
    all_gather x1, blocking collectives, per_device(): lax.all_gather(stick_bias, 'sp', axis=1, tiled=True)  28.2 us
    reduce_scatter x1, waiting for transfers between devices, per_device(): lax.psum_scatter(share.astype(jnp.bfloat16), 'tp', scatter_dimension=2, t...  26.5 us
    all_to_all x1, blocking collectives, per_device(): lax.all_to_all(outgoing, 'sp', split_axis=0, concat_axis=0, tiled=True)  16.3 us
    reduce_scatter x1, waiting for transfers between devices, per_device(): lax.psum_scatter(partial_value.astype(jnp.bfloat16), 'tp', scatter_dimens...  15.6 us
    all_gather x1, waiting for transfers between devices, per_device(): d_next = lax.all_gather(sheet, 'tp')  15.6 us
    another operation x6, other arithmetic  10.7 us
    all_to_all x1, waiting for transfers between devices, per_device(): lax.all_to_all(returned, 'sp', split_axis=0, concat_axis=0, tiled=True)  10 us
  transfers between devices with their start and end apart: 6, of which 6 were waited for; matrix products, arithmetic and copies ran while one was open for 4% of the time, Pallas kernels for 0%

profile of v1, /device:TPU:0, one launch (start us, length us, event | category | flops | bytes accessed | tf_op | source)
XLA Modules:
  0.0 250.0 jit_solution(13687845225394225698)
XLA Ops:
  6.5 1.2 copy.37
  7.8 0.7 mul.146
  8.4 0.1 mul.147
  8.5 0.8 fusion.52
  9.3 0.0 all-gather.5.cloned.1.call-start
  9.4 1.7 copy.36
  11.1 0.0 reduce-scatter.3.cloned.1.call-start
  11.1 1.0 copy.38
  12.1 0.8 copy.40
  12.9 0.1 eq.29
  13.1 0.6 reduce-window.24
  13.7 28.2 %all_gather.17 = bf16[8,1024]{1,0:T(8,128)(2,1)S(1)} all-gather(bf16[8,128]{1,0:T(8,128)(2,1)} %param.20), channel_id=1, replica_groups=mesh['sp'=8,'tp'=4] {'sp'}, dimensions={1}, use_global_device_ids=true | all-gather | bytes 18432 | tf_op jit(solution)/shard_map/all_gather | solution.py:93
  42.0 0.7 multiply_convert_fusion
  42.7 8.9 %all-gather.7.cloned.1.call-done = bf16[1024,512]{0,1:T(8,128)(2,1)} async-done(((bf16[128,512]{0,1:T(8,128)(2,1)}), bf16[1024,512]{0,1:T(8,128)(2,1)}) %all-gather.7.cloned.1.call-update) | async-done | bytes 1048592 | tf_op jit(solution)/shard_map/all_gather | solution.py:91
  51.6 40.3 %all-gather.5.cloned.1.call-done = bf16[1024,512]{0,1:T(8,128)(2,1)} async-done(((bf16[128,512]{0,1:T(8,128)(2,1)}), bf16[1024,512]{0,1:T(8,128)(2,1)}) %all-gather.5.cloned.1.call-update) | async-done | bytes 1048592 | tf_op jit(solution)/shard_map/all_gather | solution.py:92
  91.9 33.3 %while.16 = (s32[]{:T(128)}, f32[128,8,64]{0,2,1:T(8,128)S(1)}, f32[8,128]{1,0:T(8,128)S(1)}, bf16[1024,512]{0,1:T(8,128)(2,1)}, bf16[1024,512]{0,1:T(8,128)(2,1...) while((s32[]{:T(128)}, f32[128,8,64]{0,2,1:T(8,128)S(1)}, ...), condition=%wide.region_6.7_spmd.clone, body=%wide.region_2.6_spmd.clone.sunk | while | flops 219436672 | bytes 27240652 | solution.py:111
  91.9 1.3 constant_dynamic-slice_fusion.3
  93.2 0.2 compare_and_fusion.2
  93.4 3.0 %fusion.93 = (f32[8,128]{1,0:T(8,128)S(1)}, f32[8,128,512]{1,2,0:T(8,128)S(1)}, f32[8,512,128]{2,1,0:T(8,128)}) fusion(f32[8,512]{1,0:T(8,128)S(1)} %dynamic-slice_convert_fusion.2, pred[128,512]{0,1:T(8,128)(4,1)S(1)} %compare_and_fusion.2, bf16[512,8,64]{0,2,1:T(8,128)(2,1)S(1)} %bitcast.121, bf16[128,8,64]{0,2,1:T(8,128)(2,1)S(1)} %get-tuple-element.292), kind=kOutput, calls=%fused_computation.39.clone.1 | convolution fusion | flops 72875008 | bytes 4935680 | tf_op jit(solution)/shard_map/while/body/eval_jaxpr/qhd,khd->hqk/dot_general | solution.py:42
  96.4 5.0 %fusion.94 = f32[8,128,4,128]{1,0,3,2:T(8,128)S(1)} fusion(f32[8,128,4,128]{1,3,2,0:T(8,128)S(1)} %bitcast.119), kind=kOutput, calls=%fused_computation.23.clone.1 | output fusion | flops 66584576 | bytes 4194304 | tf_op jit(solution)/shard_map/reduce-window.6
  101.5 0.1 broadcast_add_fusion.2
  101.6 1.7 copy.51
  103.3 4.8 %fusion.97 = bf16[8,128,512]{1,2,0:T(8,128)(2,1)S(1)} fusion(f32[8,128,4,128]{1,3,2,0:T(8,128)} %copy.51, f32[8,512,128]{2,1,0:T(8,128)} %get-tuple-element.259, f32[8,128]{1,0:T(8,128)S(1)} %get-tuple-element.261, f32[8,512]{1,0:T(8,128)S(1)} %dynamic-slice_convert_fusion.2, pred[128,512]{0,1:T(8,128)(4,1)S(1)} %compare_and_fusion.2), kind=kLoop, calls=%fused_computation.12.clone.1 | loop fusion | flops 12058624 | bytes 5328896 | tf_op jit(solution)/shard_map/while/body/eval_jaxpr/convert_element_type | solution.py:55
  108.1 0.3 fusion.98
  108.5 1.3 constant_dynamic-slice_fusion.3
  109.8 0.2 compare_and_fusion.2
  110.1 3.0 %fusion.93 = (f32[8,128]{1,0:T(8,128)S(1)}, f32[8,128,512]{1,2,0:T(8,128)S(1)}, f32[8,512,128]{2,1,0:T(8,128)}) fusion(f32[8,512]{1,0:T(8,128)S(1)} %dynamic-slice_convert_fusion.2, pred[128,512]{0,1:T(8,128)(4,1)S(1)} %compare_and_fusion.2, bf16[512,8,64]{0,2,1:T(8,128)(2,1)S(1)} %bitcast.121, bf16[128,8,64]{0,2,1:T(8,128)(2,1)S(1)} %get-tuple-element.292), kind=kOutput, calls=%fused_computation.39.clone.1 | convolution fusion | flops 72875008 | bytes 4935680 | tf_op jit(solution)/shard_map/while/body/eval_jaxpr/qhd,khd->hqk/dot_general | solution.py:42
  113.1 5.0 %fusion.94 = f32[8,128,4,128]{1,0,3,2:T(8,128)S(1)} fusion(f32[8,128,4,128]{1,3,2,0:T(8,128)S(1)} %bitcast.119), kind=kOutput, calls=%fused_computation.23.clone.1 | output fusion | flops 66584576 | bytes 4194304 | tf_op jit(solution)/shard_map/reduce-window.6
  118.1 0.1 broadcast_add_fusion.2
  118.3 1.7 copy.51
  120.0 4.8 %fusion.97 = bf16[8,128,512]{1,2,0:T(8,128)(2,1)S(1)} fusion(f32[8,128,4,128]{1,3,2,0:T(8,128)} %copy.51, f32[8,512,128]{2,1,0:T(8,128)} %get-tuple-element.259, f32[8,128]{1,0:T(8,128)S(1)} %get-tuple-element.261, f32[8,512]{1,0:T(8,128)S(1)} %dynamic-slice_convert_fusion.2, pred[128,512]{0,1:T(8,128)(4,1)S(1)} %compare_and_fusion.2), kind=kLoop, calls=%fused_computation.12.clone.1 | loop fusion | flops 12058624 | bytes 5328896 | tf_op jit(solution)/shard_map/while/body/eval_jaxpr/convert_element_type | solution.py:55
  124.8 0.3 fusion.98
  125.2 2.9 %convolution_convert_fusion.1 = bf16[128,2048]{1,0:T(8,128)(2,1)} fusion(bf16[128,512]{0,1:T(8,128)(2,1)S(1)} %bitcast.126, bf16[512,2048]{1,0:T(8,128)(2,1)} %param.23), kind=kOutput, calls=%fused_computation.41 | convolution fusion | flops 268697600 | bytes 2752512 | tf_op jit(solution)/shard_map/dot_general | solution.py:113
  128.1 0.0 all-gather.9.cloned.1.call-start
  128.1 0.2 slice_reduce_fusion
  128.3 0.1 eq.25
  128.5 0.1 copy.39
  128.6 0.1 mul.162
  128.8 0.1 fusion.58
  128.9 1.4 scatter_custom_fusion
  130.3 2.2 scatter_custom_fusion.1
  132.5 0.1 mul.164
  132.6 0.8 dynamic_slice.28
  133.3 15.6 %reduce-scatter.3.cloned.1.call-done = bf16[128,512]{1,0:T(8,128)(2,1)} async-done(((bf16[128,2048]{1,0:T(8,128)(2,1)}), bf16[128,512]{1,0:T(8,128)(2,1)}) %reduce-scatter.3.cloned.1.call-update) | async-done | bytes 131088 | tf_op jit(solution)/shard_map/reduce_scatter | solution.py:133
  148.9 1.1 fusion.53
  150.0 5.8 %psum.7 = f32[128]{0:T(128)S(1)} all-reduce(f32[128]{0:T(128)S(1)} %get-tuple-element.193), channel_id=1, replica_groups=mesh['sp'=8,'tp'=4] {'tp'}, use_global_device_ids=true, to_apply=%region_9.10 | all-reduce | flops 128 | bytes 1024 | tf_op jit(solution)/shard_map/psum | solution.py:140
  155.8 0.1 fusion.55
  155.9 2.0 gather_fusion
  157.9 0.1 broadcast_multiply_fusion
  158.0 16.3 %all_to_all.10 = bf16[8,40,512]{2,1,0:T(8,128)(2,1)} all-to-all(bf16[8,40,512]{2,1,0:T(8,128)(2,1)S(1)} %broadcast_multiply_fusion), channel_id=1, replica_groups=mesh['sp'=8,'tp'=4] {'sp'}, dimensions={0} | all-to-all | bytes 655360 | tf_op jit(solution)/shard_map/all_to_all | solution.py:146
  174.4 0.2 reduce-scatter.5.cloned.1.call-start
  174.6 15.6 %all-gather.9.cloned.1.call-done = bf16[32,40,512]{2,1,0:T(8,128)(2,1)} async-done(((bf16[8,40,512]{2,1,0:T(8,128)(2,1)}), bf16[32,40,512]{2,1,0:T(8,128)(2,1)}) %all-gather.9.cloned.1.call-update) | async-done | bytes 1310736 | tf_op jit(solution)/shard_map/all_gather | solution.py:147
  190.1 1.6 copy.45
  191.8 0.3 copy-done.3
  192.1 1.8 fusion.33
  193.9 4.5 %convolution_convert_fusion = bf16[8,40,2048]{2,1,0:T(8,128)(2,1)} fusion(bf16[1,512,2048]{2,1,0:T(8,128)(2,1)S(1)} %copy-done, bf16[8,40,2048]{2,1,0:T(8,128)(2,1)S(1)} %bitcast.125, bf16[1,2048,512]{2,1,0:T(8,128)(2,1)} %param.28, f32[8,40,512]{2,1,0:T(8,128)} %fusion.33), kind=kOutput, calls=%fused_computation.40 | convolution fusion | flops 1344307200 | bytes 7471104 | tf_op jit(solution)/shard_map/scf,fd->scd/dot_general | solution.py:152
  198.4 26.5 %reduce-scatter.5.cloned.1.call-done = bf16[8,40,512]{2,1,0:T(8,128)(2,1)} async-done(((bf16[8,40,2048]{2,1,0:T(8,128)(2,1)}), bf16[8,40,512]{2,1,0:T(8,128)(2,1)}) %reduce-scatter.5.cloned.1.call-update) | async-done | bytes 327696 | tf_op jit(solution)/shard_map/reduce_scatter | solution.py:153
  224.9 5.5 %all-to-all-start.1 = ((bf16[8,40,512]{2,1,0:T(8,128)(2,1)}), bf16[8,40,512]{2,1,0:T(8,128)(2,1)S(1)}, u32[]{:S(2)}, u32[]{:S(2)}) async-start(bf16[8,40,512]{2,1,0:T(8,128)(2,1)} %reduce-scatter.5.cloned.1.call-done), calls=%async_computation.3 | async-start | bytes 655360 | tf_op jit(solution)/shard_map/all_to_all | solution.py:154
  230.4 0.1 copy.43
  230.6 10.0 %all-to-all-done.1 = bf16[8,40,512]{2,1,0:T(8,128)(2,1)S(1)} async-done(((bf16[8,40,512]{2,1,0:T(8,128)(2,1)}), bf16[8,40,512]{2,1,0:T(8,128)(2,1)S(1)}, u32[]{:S(2)}, u32[]{:S(2)}) %all-to-all-start.1) | async-done | bytes 327712 | tf_op jit(solution)/shard_map/all_to_all | solution.py:154
  240.6 1.2 gather_fusion.1
  241.7 0.3 reshape.196
  242.1 0.7 multiply_reduce_fusion
  242.8 0.7 fusion.56
  (45 shorter events, 0.4 us)
Async XLA Ops:
  6.5 187.3 %copy-start = (bf16[1,512,2048]{2,1,0:T(8,128)(2,1)S(1)}, bf16[1,512,2048]{2,1,0:T(8,128)(2,1)}, u32[]{:S(2)}) copy-start(bf16[1,512,2048]{2,1,0:T(8,128)(2,1)} %param.29) | copy-start | bytes 6291460
  6.5 45.1 %all-gather.7.cloned.1.call-start = ((), (), s32[]{:S(2)}) async-start(), calls=%async_computation.5 | async-start | bytes 1179648 | tf_op jit(solution)/shard_map/all_gather | solution.py:91
  9.3 82.6 %all-gather.5.cloned.1.call-start = ((), (), s32[]{:S(2)}) async-start(), calls=%async_computation.4 | async-start | bytes 1179648 | tf_op jit(solution)/shard_map/all_gather | solution.py:92
  11.1 137.9 %reduce-scatter.3.cloned.1.call-start = ((), (), s32[]{:S(2)}) async-start(), calls=%async_computation.6 | async-start | bytes 655360 | tf_op jit(solution)/shard_map/reduce_scatter | solution.py:133
  125.1 3.4 %copy-start.1 = (s32[128,2]{0,1:T(2,128)S(1)}, s32[128,2]{0,1:T(2,128)}, u32[]{:S(2)}) copy-start(s32[128,2]{0,1:T(2,128)} %param.25) | copy-start | bytes 3076
  128.1 62.1 %all-gather.9.cloned.1.call-start = ((), (), s32[]{:S(2)}) async-start(), calls=%async_computation.8 | async-start | bytes 1638400 | tf_op jit(solution)/shard_map/all_gather | solution.py:147
  174.4 50.6 %reduce-scatter.5.cloned.1.call-start = ((), (), s32[]{:S(2)}) async-start(), calls=%async_computation.7 | async-start | bytes 1638400 | tf_op jit(solution)/shard_map/reduce_scatter | solution.py:153
  190.1 2.0 copy-start.3
  193.9 36.5 %copy-start.2 = (f32[128,2]{0,1:T(2,128)S(1)}, f32[128,2]{0,1:T(2,128)}, u32[]{:S(2)}) copy-start(f32[128,2]{0,1:T(2,128)} %param.26) | copy-start | bytes 3076
  224.9 15.7 %all-to-all-start.1 = ((bf16[8,40,512]{2,1,0:T(8,128)(2,1)}), bf16[8,40,512]{2,1,0:T(8,128)(2,1)S(1)}, u32[]{:S(2)}, u32[]{:S(2)}) async-start(bf16[8,40,512]{2,1,0:T(8,128)(2,1)} %reduce-scatter.5.cloned.1.call-done), calls=%async_computation.3 | async-start | bytes 655360 | tf_op jit(solution)/shard_map/all_to_all | solution.py:154
Sparse Core Ops, SparseCore 0:
  9.4 42.1 all-gather.6
  53.6 38.1 all-gather.4
  128.2 20.6 reduce-scatter.2
  174.5 15.6 all-gather.8
  198.5 26.3 reduce-scatter.4
